TPU v7x, 32 devices: a whole 2x2x4 slice. The times are simulated.
32 devices in a mesh: grp: 2 (over y), sp: 4 (over z), tp: 4 (over x, core).
Axes of the slice: x: 2, y: 2, z: 4, core: 2. Of those that a mesh axis runs over, the one named last changes fastest.
Arguments:
- tokens_in: bfloat16 [2048, 2048], P(('grp', 'sp')), parts along dimension 0, may hold values from -6 to 6
- input_gain: float32 [2048], replicated, may hold values from 0.1 to 1.9
- w_query: bfloat16 [2048, 1024], P('sp', 'tp'), may hold values from -0.125 to 0.125
- w_key: bfloat16 [2048, 1024], P('sp', 'tp'), may hold values from -1 to 1
- w_value: bfloat16 [2048, 1024], P('sp', 'tp'), may hold values from -0.125 to 0.125
- w_gates: bfloat16 [2048, 32], P('sp', 'tp'), may hold values from -3 to 3
- w_glu_value: bfloat16 [2048, 1024], P('sp', 'tp'), may hold values from -0.125 to 0.125
- sigmoid_opener_matrix: bfloat16 [2048, 1024], P('sp', 'tp'), may hold values from -0.125 to 0.125
- log_decay: float32 [2048, 16], P(('grp', 'sp'), 'tp'), parts along dimension 0, may hold values from -1 to 0
- head_gain: float32 [128], replicated, may hold values from 0.1 to 1.9
- conv_kernel: float32 [31, 1024], P(None, 'tp'), may hold values from -12 to 12
- norm_gain: float32 [1024], P('tp'), may hold values from 0.1 to 1.9
- norm_shift: float32 [1024], P('tp'), may hold values from -3 to 3
- out_delta: bfloat16 [2048, 1024], P(None, 'tp'), may hold values from -0.125 to 0.125
- out_conv: bfloat16 [2048, 1024], P(None, 'tp'), may hold values from -0.125 to 0.125
Outputs:
- mixed: bfloat16 [2048, 2048], P(('grp', 'sp'), 'tp'), parts along dimension 0
There are 2 independent parts, one for each index of `grp`. A program takes and returns all parts, laid end to end along the dimension named above; an argument that names none is the same for every part. Nothing has to cross between parts.
All inputs are finite; a program needn't handle non-finite values.
Results may differ from a plain program's by a relative error of at most 0.015.
Values may be sent and summed in bfloat16 or wider, within the bound.
A program may use at most 64 MiB of HBM per device.

v0:
```python
import jax
import jax.numpy as jnp
from jax import lax
from jax.sharding import PartitionSpec as P

CONV_CH = 1024
BLOCK = 64


PRECISE = lax.Precision.HIGHEST
EPSILON = 1e-06
BETA_SHIFT = 6.0


def entering(value, axis, combine, identity, reverse):
    devices, place = (lax.axis_size(axis), lax.axis_index(axis))
    everything = jax.tree.map(
        lambda part, kind: lax.all_gather(part.astype(kind), axis),
        value,
        (jnp.bfloat16, jnp.bfloat16),
    )
    start = jax.tree.map(
        lambda part, zero: jnp.broadcast_to(jnp.asarray(zero, part.dtype), part.shape),
        value,
        identity,
    )

    def lap(k, before):
        at = devices - 1 - k if reverse else k
        reached = at > place if reverse else at < place
        new = combine(
            before, jax.tree.map(lambda part, own: part[at].astype(own.dtype), everything, value)
        )
        return jax.tree.map(lambda a, b: jnp.where(reached, a, b), new, before)

    return lax.fori_loop(0, devices, lap, start)


def with_halo(block, sides, width):
    for axis, dim in sides:
        count = lax.axis_size(axis)
        forward = [(i, i + 1) for i in range(count - 1)]
        backward = [(target, source) for source, target in forward]
        low = lax.ppermute(
            lax.slice_in_dim(block, block.shape[dim] - width, None, axis=dim), axis, forward
        )
        high = lax.ppermute(lax.slice_in_dim(block, 0, width, axis=dim), axis, backward)
        block = jnp.concatenate([low, block, high], axis=dim)
    return block


def high_dot(left, right):
    return jnp.matmul(left, right, precision=PRECISE)


def swap_last(tensor):
    return jnp.swapaxes(tensor, -1, -2)


def block_terms(query, key_rows, values, decay_log, beta_rate, block):
    head_count, length = (query.shape[0], query.shape[1])
    blocks = length // block

    def to_blocks(tensor):
        return tensor.reshape((head_count, blocks, block) + tensor.shape[2:])

    query, key_rows, values, decay_log, beta_rate = (
        to_blocks(tensor) for tensor in (query, key_rows, values, decay_log, beta_rate)
    )
    cumulative = jnp.cumsum(decay_log, axis=-1)
    positions = jnp.arange(block)
    on_or_below = positions[:, None] >= positions[None, :]
    strict = positions[:, None] > positions[None, :]
    log_gaps = cumulative[..., :, None] - cumulative[..., None, :]
    weighting = jnp.where(on_or_below, jnp.exp(jnp.where(on_or_below, log_gaps, 0.0)), 0.0)
    scaled_keys = key_rows * beta_rate[..., None]
    lower_part = jnp.where(strict, high_dot(scaled_keys, swap_last(key_rows)) * weighting, 0.0)
    identity = jnp.eye(block, dtype=jnp.float32)
    inverse = jax.scipy.linalg.solve_triangular(
        identity + lower_part,
        jnp.broadcast_to(identity, lower_part.shape),
        lower=True,
        unit_diagonal=True,
    )
    update = high_dot(inverse, values * beta_rate[..., None])
    mixed_keys = high_dot(inverse, scaled_keys * jnp.exp(cumulative)[..., None])
    in_block = jnp.where(on_or_below, high_dot(query, swap_last(key_rows)) * weighting, 0.0)
    q_decayed = query * jnp.exp(cumulative)[..., None]
    k_decayed = key_rows * jnp.exp(cumulative[..., -1:] - cumulative)[..., None]
    end_decay = jnp.exp(cumulative[..., -1])
    return tuple(
        (
            jnp.moveaxis(tensor, 1, 0)
            for tensor in (update, mixed_keys, in_block, q_decayed, k_decayed, end_decay)
        )
    )


def delta_local(query, key_rows, values, decay_log, beta_rate):
    stacked = block_terms(query, key_rows, values, decay_log, beta_rate, BLOCK)
    head_count, length, head_width = query.shape
    identity = jnp.broadcast_to(
        jnp.eye(head_width, dtype=jnp.float32), (head_count, head_width, head_width)
    )
    zero_state = jnp.zeros((head_count, head_width, values.shape[2]), jnp.float32)

    def advance(carry, pieces):
        state_now, carried = carry
        update, mixed_keys, in_block, q_decayed, k_decayed, end_decay = pieces
        new_values = update - high_dot(mixed_keys, state_now)
        output = high_dot(q_decayed, state_now) + high_dot(in_block, new_values)
        reading = high_dot(q_decayed - high_dot(in_block, mixed_keys), carried)
        passing = end_decay[:, None, None] * identity - high_dot(swap_last(k_decayed), mixed_keys)
        state_now = state_now * end_decay[:, None, None] + high_dot(
            swap_last(k_decayed), new_values
        )
        return ((state_now, high_dot(passing, carried)), (output, reading))

    (state_now, carried), (output, reading) = lax.scan(advance, (zero_state, identity), stacked)
    output = jnp.moveaxis(output, 0, 1).reshape(head_count, length, values.shape[2])
    reading = jnp.moveaxis(reading, 0, 1).reshape(head_count, length, head_width)
    return (output, reading, carried, state_now)


def chain(earlier, later):
    return (high_dot(later[0], earlier[0]), high_dot(later[0], earlier[1]) + later[1])


def reversed_rows(tensor):
    return jnp.flip(tensor, axis=1)


def delta_branch(query_proj, key_proj, value_proj, gate_proj, log_decay, head_gain):
    head_width = head_gain.shape[0]
    length = query_proj.shape[0]
    head_count = query_proj.shape[1] // head_width

    def by_head(tensor):
        return jnp.swapaxes(jax.nn.silu(tensor).reshape(length, head_count, head_width), 0, 1)

    def unit_rows(tensor):
        return tensor * lax.rsqrt(jnp.sum(tensor * tensor, axis=-1, keepdims=True) + EPSILON)

    query = unit_rows(by_head(query_proj)) * head_width ** (-0.5)
    key_rows = unit_rows(by_head(key_proj))
    values = by_head(value_proj)
    gate_parts = gate_proj.reshape(length, head_count, 4)
    rate_parts = log_decay.reshape(length, head_count, 2)
    decay_fore = jnp.swapaxes(
        rate_parts[:, :, 0] * (0.5 + jax.nn.sigmoid(gate_parts[:, :, 0])), 0, 1
    )
    beta_fore = jnp.swapaxes(jax.nn.sigmoid(gate_parts[:, :, 1] - BETA_SHIFT), 0, 1)
    decay_back = jnp.swapaxes(
        rate_parts[:, :, 1] * (0.5 + jax.nn.sigmoid(gate_parts[:, :, 2])), 0, 1
    )
    beta_back = jnp.swapaxes(jax.nn.sigmoid(gate_parts[:, :, 3] - BETA_SHIFT), 0, 1)
    identity = jnp.broadcast_to(
        jnp.eye(head_width, dtype=jnp.float32), (head_count, head_width, head_width)
    )
    zero_state = jnp.zeros((head_count, head_width, head_width), jnp.float32)
    forward_out, forward_read, forward_map, forward_end = delta_local(
        query, key_rows, values, decay_fore, beta_fore
    )
    forward_start = entering(
        (forward_map, forward_end), "sp", chain, (identity, zero_state), False
    )[1]
    back_out, back_read, back_map, back_end = delta_local(
        reversed_rows(query),
        reversed_rows(key_rows),
        reversed_rows(values),
        reversed_rows(decay_back),
        reversed_rows(beta_back),
    )
    back_start = entering((back_map, back_end), "sp", chain, (identity, zero_state), True)[1]
    joined = forward_out + high_dot(forward_read, forward_start)
    joined = joined + reversed_rows(back_out + high_dot(back_read, back_start))
    joined = (
        joined * lax.rsqrt(jnp.mean(joined * joined, axis=-1, keepdims=True) + EPSILON) * head_gain
    )
    return jnp.swapaxes(joined, 0, 1).reshape(length, head_count * head_width).astype(jnp.bfloat16)


def conv_branch(value_proj, gate_proj, conv_kernel, norm_gain, norm_shift):
    glu_rows = (value_proj * jax.nn.sigmoid(gate_proj)).astype(jnp.bfloat16)
    half_width = conv_kernel.shape[0] // 2
    length = glu_rows.shape[0]
    padded = with_halo(glu_rows, (("sp", 0),), half_width).astype(jnp.float32)
    conv_rows = padded[0:length] * conv_kernel[0]
    for offset in range(1, conv_kernel.shape[0]):
        conv_rows = conv_rows + padded[offset : offset + length] * conv_kernel[offset]
    row_sum, row_squares = lax.psum(
        (jnp.sum(conv_rows, axis=-1), jnp.sum(conv_rows * conv_rows, axis=-1)), "tp"
    )
    center = row_sum / CONV_CH
    spread = row_squares / CONV_CH - center * center
    normal_rows = (conv_rows - center[:, None]) * lax.rsqrt(spread + EPSILON)[:, None]
    return jax.nn.silu(normal_rows * norm_gain + norm_shift).astype(jnp.bfloat16)


def on_device(
    tokens_in,
    input_gain,
    w_query,
    w_key,
    w_value,
    w_gates,
    w_glu_value,
    sigmoid_opener_matrix,
    log_decay,
    head_gain,
    conv_kernel,
    norm_gain,
    norm_shift,
    out_delta,
    out_conv,
):
    rows = tokens_in.astype(jnp.float32)
    normed = (
        rows * lax.rsqrt(jnp.mean(rows * rows, axis=-1, keepdims=True) + EPSILON) * input_gain
    ).astype(jnp.bfloat16)
    weight_rows = (
        lax.all_gather(w_query, "sp", axis=0, tiled=True),
        lax.all_gather(w_key, "sp", axis=0, tiled=True),
        lax.all_gather(w_value, "sp", axis=0, tiled=True),
        lax.all_gather(w_gates, "sp", axis=0, tiled=True),
        lax.all_gather(w_glu_value, "sp", axis=0, tiled=True),
        lax.all_gather(sigmoid_opener_matrix, "sp", axis=0, tiled=True),
    )
    projected = tuple(
        (
            jnp.dot(normed, rows_here, preferred_element_type=jnp.float32)
            for rows_here in weight_rows
        )
    )
    delta_mix = delta_branch(
        projected[0], projected[1], projected[2], projected[3], log_decay, head_gain
    )
    filtered_blend = conv_branch(projected[4], projected[5], conv_kernel, norm_gain, norm_shift)
    contract = (((1,), (1,)), ((), ()))
    term = lax.dot_general(delta_mix, out_delta, contract, preferred_element_type=jnp.float32)
    term = term + lax.dot_general(
        filtered_blend, out_conv, contract, preferred_element_type=jnp.float32
    )
    return lax.psum_scatter(term.astype(jnp.bfloat16), "tp", scatter_dimension=1, tiled=True)


def solution(mesh):
    placed = (
        P(("grp", "sp"), None),
        P(),
        P("sp", "tp"),
        P("sp", "tp"),
        P("sp", "tp"),
        P("sp", "tp"),
        P("sp", "tp"),
        P("sp", "tp"),
        P(("grp", "sp"), "tp"),
        P(),
        P(None, "tp"),
        P("tp"),
        P("tp"),
        P(None, "tp"),
        P(None, "tp"),
    )
    return jax.shard_map(
        on_device, mesh=mesh, in_specs=placed, out_specs=P(("grp", "sp"), "tp"), check_vma=False
    )
```

profile of v0, /device:TPU:0, one launch (start us, length us, event | category | flops | bytes accessed | tf_op | source)
XLA Modules:
  0.0 307.7 jit_solution(15829972649994109252)
XLA Ops:
  10.4 14.9 %all_gather.42 = bf16[2048,8]{0,1:T(8,128)(2,1)S(1)} all-gather(bf16[512,8]{0,1:T(8,128)(2,1)S(1)} %copy-done.10), channel_id=1, replica_groups=mesh['grp'=2,'sp'=4,'tp'=4] {'sp'}, dimensions={0}, use_global_device_ids=true | all-gather | bytes 40960 | tf_op jit(solution)/shard_map/all_gather | solution.py:225
  30.7 9.1 %all-gather.10.cloned.1.call-done = bf16[2048,256]{1,0:T(8,128)(2,1)} async-done(((bf16[512,256]{1,0:T(8,128)(2,1)}), bf16[2048,256]{1,0:T(8,128)(2,1)}) %all-gather.10.cloned.1.call-update) | async-done | bytes 1048592 | tf_op jit(solution)/shard_map/all_gather | solution.py:223
  39.8 1.9 divide_multiply_fusion.2
  43.0 39.3 %custom-call.8 = f32[2,4,1,64,64]{3,4,2,1,0:T(8,128)S(1)} custom-call(f32[2,4,1,64,64]{4,3,2,1,0:T(8,128)S(1)} %fusion.104), custom_call_target="InvertDiagBlocksLowerTriangular" | custom-call | tf_op jit(solution)/shard_map/jit(_solve_triangular)/vmap(vmap())/triangular_solve | solution.py:79
  82.9 2.2 divide_multiply_fusion.1
  85.9 1.1 convolution_bitcast_fusion.7
  87.2 10.9 %all-gather.14.cloned.1.call-done = bf16[2048,256]{1,0:T(8,128)(2,1)} async-done(((bf16[512,256]{1,0:T(8,128)(2,1)}), bf16[2048,256]{1,0:T(8,128)(2,1)}) %all-gather.14.cloned.1.call-update) | async-done | bytes 1048592 | tf_op jit(solution)/shard_map/all_gather | solution.py:222
  98.1 2.2 divide_multiply_fusion
  100.6 0.8 broadcast_multiply_fusion.1
  103.6 20.2 %while.64 = (s32[]{:T(128)}, f32[2,128,128]{2,1,0:T(8,128)S(1)}, f32[2,128,128]{2,1,0:T(8,128)S(1)}, f32[4,2,64,128]{3,2,0,1:T(8,128)}, f32[4,2,64,128]{3,2,0,1:...) while((s32[]{:T(128)}, f32[2,128,128]{2,1,0:T(8,128)S(1)}, ...), condition=%wide.region_5.7_spmd.clone, body=%wide.region_4.6_spmd.clone.sunk | while | flops 201605120 | bytes 2758829 | solution.py:119
  103.6 1.1 convolution_subtract_fusion.12
  104.9 0.8 fusion.320
  107.1 0.9 fusion.321
  108.6 1.1 convolution_subtract_fusion.12
  110.0 0.8 fusion.320
  112.1 0.9 fusion.321
  113.7 1.1 convolution_subtract_fusion.12
  115.0 0.8 fusion.320
  117.1 0.9 fusion.321
  118.7 1.1 convolution_subtract_fusion.12
  120.0 0.8 fusion.320
  122.2 0.9 fusion.321
  123.8 14.6 %all-gather = bf16[8,128,128]{2,1,0:T(8,128)(2,1)} all-gather(bf16[2,128,128]{2,1,0:T(8,128)(2,1)S(1)} %convert_element_type.96), channel_id=2, replica_groups=mesh['grp'=2,'sp'=4,'tp'=4] {'sp'}, dimensions={0}, use_global_device_ids=true | all-gather | bytes 327680 | tf_op jit(solution)/shard_map/all_gather | solution.py:18
  138.4 17.3 %all-gather.1 = bf16[8,128,128]{2,1,0:T(8,128)(2,1)} all-gather(bf16[2,128,128]{2,1,0:T(8,128)(2,1)S(1)} %convert_element_type.97), channel_id=3, replica_groups=mesh['grp'=2,'sp'=4,'tp'=4] {'sp'}, dimensions={0}, use_global_device_ids=true | all-gather | bytes 327680 | tf_op jit(solution)/shard_map/all_gather | solution.py:18
  155.7 1.8 copy.93
  158.1 39.3 %custom-call.9 = f32[2,4,1,64,64]{3,4,2,1,0:T(8,128)S(1)} custom-call(f32[2,4,1,64,64]{4,3,2,1,0:T(8,128)S(1)} %fusion.108), custom_call_target="InvertDiagBlocksLowerTriangular" | custom-call | tf_op jit(solution)/shard_map/jit(_solve_triangular)/vmap(vmap())/triangular_solve | solution.py:79
  201.0 14.3 %while.66 = (s32[]{:T(128)}, f32[2,128,128]{2,1,0:T(8,128)S(1)}, f32[2,128,128]{2,1,0:T(8,128)S(1)}, f32[4,2,64,128]{3,2,0,1:T(8,128)}, f32[4,2,64,128]{3,2,0,1:...) while((s32[]{:T(128)}, f32[2,128,128]{2,1,0:T(8,128)S(1)}, ...), condition=%wide.region_10.12_spmd.clone, body=%wide.region_9.11_spmd.clone.sunk | while | flops 201605120 | bytes 2758321 | solution.py:119
  201.5 0.8 fusion.344
  205.1 0.8 fusion.344
  208.7 0.8 fusion.344
  212.3 0.8 fusion.344
  215.4 14.0 %all-gather.2 = bf16[8,128,128]{2,1,0:T(8,128)(2,1)S(1)} all-gather(bf16[2,128,128]{2,1,0:T(8,128)(2,1)S(1)} %convert_element_type.98), channel_id=4, replica_groups=mesh['grp'=2,'sp'=4,'tp'=4] {'sp'}, dimensions={0}, use_global_device_ids=true | all-gather | bytes 327680 | tf_op jit(solution)/shard_map/all_gather | solution.py:18
  229.4 13.9 %all-gather.3 = bf16[8,128,128]{2,1,0:T(8,128)(2,1)S(1)} all-gather(bf16[2,128,128]{2,1,0:T(8,128)(2,1)S(1)} %convert_element_type.99), channel_id=5, replica_groups=mesh['grp'=2,'sp'=4,'tp'=4] {'sp'}, dimensions={0}, use_global_device_ids=true | all-gather | bytes 327680 | tf_op jit(solution)/shard_map/all_gather | solution.py:18
  243.3 1.1 while.67
  245.4 4.7 %while.65 = (s32[]{:T(128)}, f32[2,128,128]{2,1,0:T(8,128)S(1)}, s32[]{:T(128)}, bf16[4,2,128,128]{3,2,1,0:T(8,128)(2,1)}, bf16[4,2,128,128]{3,2,1,0:T(8,128)(2,1)}, /*index=5*/s32[]{:T(128)}, s32[]{:T(128)}) while((s32[]{:T(128)}, f32[2,128,128]{2,1,0:T(8,128)S(1)}, s32[]{:T(128)}, bf16[4,2,128,128]{3,2,1,0:T(8,128)(2,1)}, ...), condition=%wide.region_7.9_spmd.clone, body=%wide.region_6.8_spmd.clone.sunk | while | flops 50495492 | bytes 789087 | solution.py:36
  245.5 1.2 fusion.324
  246.7 1.1 fusion.324
  247.8 1.1 fusion.324
  249.0 1.1 fusion.324
  250.6 1.9 fusion.192
  252.6 1.9 fusion.113
  254.6 2.5 collective-permute-start
  257.1 1.3 collective-permute-start.1
  259.3 3.9 %collective-permute-done.1 = bf16[15,256]{0,1:T(8,128)(2,1)S(1)} collective-permute-done((bf16[15,256]{0,1:T(8,128)(2,1)S(1)}, bf16[15,256]{0,1:T(8,128)(2,1)S(1)}, u32[]{:S(2)}, u32[]{:S(2)}) %collective-permute-start.1) | collective-permute-done | bytes 7712 | tf_op jit(solution)/shard_map/ppermute | solution.py:47
  263.7 3.5 %fusion.208 = (f32[256]{0:T(256)S(1)}, f32[256]{0:T(256)S(1)}, f32[256,256]{0,1:T(8,128)S(1)}) fusion(f32[256]{0:T(256)S(1)} %bitcast.421, f32[286,256]{0,1:T(8,128)S(1)} %maximum_convert_fusion, f32[256]{0:T(256)S(1)} %bitcast.422, f32[256]{0:T(256)S(1)} %bitcast.393, f32[256]{0:T(256)S(1)} %bitcast.394, f32[256]{0:T(256)S(1)} %bitcast.395, ...), kind=kLoop, calls=%fused_computation.302 | loop fusion | flops 4193792 | bytes 8422400 | tf_op jit(solution)/shard_map/reduce_sum | solution.py:192
  267.2 5.7 %all-reduce = (f32[256]{0:T(256)S(1)}, f32[256]{0:T(256)S(1)}) all-reduce(f32[256]{0:T(256)S(1)} %get-tuple-element.565, f32[256]{0:T(256)S(1)} %get-tuple-element.564), channel_id=1, replica_groups=mesh['grp'=2,'sp'=4,'tp'=4] {'tp'}, use_global_device_ids=true, to_apply=%region_17.19 | all-reduce | flops 512 | bytes 4096 | tf_op jit(solution)/shard_map/psum | solution.py:191
  272.9 2.9 fusion.90
  275.8 25.1 %reduce-scatter.2.cloned.1.call-done = bf16[256,512]{1,0:T(8,128)(2,1)} async-done(((bf16[256,2048]{1,0:T(8,128)(2,1)}), bf16[256,512]{1,0:T(8,128)(2,1)}) %reduce-scatter.2.cloned.1.call-update) | async-done | bytes 262160 | tf_op jit(solution)/shard_map/reduce_scatter | solution.py:244
  (280 shorter events, 41.1 us)
Async XLA Ops:
  6.5 252.2 %copy-start = (bf16[2048,256]{1,0:T(8,128)(2,1)S(1)}, bf16[2048,256]{1,0:T(8,128)(2,1)}, u32[]{:S(2)}) copy-start(bf16[2048,256]{1,0:T(8,128)(2,1)} %param.38) | copy-start | bytes 3145732
  6.5 18.7 %copy-start.51 = (f32[2048]{0:T(1024)S(1)}, f32[2048]{0:T(1024)}, u32[]{:S(2)}) copy-start(f32[2048]{0:T(1024)} %param.26) | copy-start | bytes 24580
  6.5 33.3 %all-gather.10.cloned.1.call-start = ((), (), s32[]{:S(2)}) async-start(), calls=%async_computation.1 | async-start | bytes 1310720 | tf_op jit(solution)/shard_map/all_gather | solution.py:223
  7.3 18.4 %copy-start.44 = (f32[256,4]{0,1:T(4,128)S(1)}, f32[256,4]{0,1:T(4,128)}, u32[]{:S(2)}) copy-start(f32[256,4]{0,1:T(4,128)} %param.33) | copy-start | bytes 12292
  7.3 75.6 %all-gather.12.cloned.1.call-start = ((), (), s32[]{:S(2)}) async-start(), calls=%async_computation.2 | async-start | bytes 1310720 | tf_op jit(solution)/shard_map/all_gather | solution.py:224
  8.0 19.6 %copy-start.9 = (f32[31,256]{1,0:T(8,128)S(1)}, f32[31,256]{1,0:T(8,128)}, u32[]{:S(2)}) copy-start(f32[31,256]{1,0:T(8,128)} %param.35) | copy-start | bytes 95236
  8.0 90.0 %all-gather.14.cloned.1.call-start = ((), (), s32[]{:S(2)}) async-start(), calls=%async_computation.3 | async-start | bytes 1310720 | tf_op jit(solution)/shard_map/all_gather | solution.py:222
  8.8 241.8 %all-gather.16.cloned.1.call-start = ((), (), s32[]{:S(2)}) async-start(), calls=%async_computation.4 | async-start | bytes 1310720 | tf_op jit(solution)/shard_map/all_gather | solution.py:226
  9.4 243.2 %all-gather.18.cloned.1.call-start = ((), (), s32[]{:S(2)}) async-start(), calls=%async_computation.5 | async-start | bytes 1310720 | tf_op jit(solution)/shard_map/all_gather | solution.py:227
  9.9 290.9 %reduce-scatter.2.cloned.1.call-start = ((), (), s32[]{:S(2)}) async-start(), calls=%async_computation.6 | async-start | bytes 1310720 | tf_op jit(solution)/shard_map/reduce_scatter | solution.py:244
  10.0 32.3 %copy-start.7 = (f32[64,64]{1,0:T(8,128)}, f32[64,64]{1,0:T(8,128)S(1)}, u32[]{:S(2)}) copy-start(f32[64,64]{1,0:T(8,128)S(1)} %fusion.171) | copy-start | bytes 49156
  10.4 72.6 %copy-start.47 = (f32[256]{0:T(256)}, f32[256]{0:T(256)S(1)}, u32[]{:S(2)}) copy-start(f32[256]{0:T(256)S(1)} %add_rsqrt_fusion.4) | copy-start | bytes 3076
  29.1 13.2 %copy-start.11 = (pred[64,64]{1,0:T(8,128)(4,1)}, pred[64,64]{1,0:T(8,128)(4,1)S(1)}, u32[]{:S(2)}) copy-start(pred[64,64]{1,0:T(8,128)(4,1)S(1)} %get-tuple-element.690) | copy-start | bytes 12292
  85.2 12.9 %copy-start.48 = (f32[256]{0:T(256)S(1)}, f32[256]{0:T(256)}, u32[]{:S(2)}) copy-start(f32[256]{0:T(256)} %copy-done.47) | copy-start | bytes 3076
  85.2 12.9 %copy-start.52 = (f32[2048]{0:T(1024)S(1)}, f32[2048]{0:T(1024)}, u32[]{:S(2)}) copy-start(f32[2048]{0:T(1024)} %param.26) | copy-start | bytes 24580
  103.6 54.0 %copy-start.8 = (f32[64,64]{1,0:T(8,128)S(1)}, f32[64,64]{1,0:T(8,128)}, u32[]{:S(2)}) copy-start(f32[64,64]{1,0:T(8,128)} %copy-done.7) | copy-start | bytes 49156
  103.6 54.0 %copy-start.12 = (pred[64,64]{1,0:T(8,128)(4,1)S(1)}, pred[64,64]{1,0:T(8,128)(4,1)}, u32[]{:S(2)}) copy-start(pred[64,64]{1,0:T(8,128)(4,1)} %copy-done.11) | copy-start | bytes 12292
  157.5 41.9 %copy-start.1 = (f32[2,256,128]{2,1,0:T(8,128)S(1)}, f32[2,256,128]{2,1,0:T(8,128)}, u32[]{:S(2)}) copy-start(f32[2,256,128]{2,1,0:T(8,128)} %get-tuple-element.638) | copy-start | bytes 786436
  229.4 15.0 %copy-start.4 = (f32[4,2,64,128]{3,2,0,1:T(8,128)S(1)}, f32[4,2,64,128]{3,2,0,1:T(8,128)}, u32[]{:S(2)}) copy-start(f32[4,2,64,128]{3,2,0,1:T(8,128)} %get-tuple-element.367) | copy-start | bytes 786436
  245.0 5.1 %copy-start.5 = (f32[2,256,128]{1,2,0:T(8,128)S(1)}, f32[2,256,128]{1,2,0:T(8,128)}, u32[]{:S(2)}) copy-start(f32[2,256,128]{1,2,0:T(8,128)} %copy.93) | copy-start | bytes 786436
  245.0 5.1 %copy-start.6 = (f32[4,2,64,128]{3,2,0,1:T(8,128)S(1)}, f32[4,2,64,128]{3,2,0,1:T(8,128)}, u32[]{:S(2)}) copy-start(f32[4,2,64,128]{3,2,0,1:T(8,128)} %get-tuple-element.363) | copy-start | bytes 786436
  245.4 5.2 %copy-start.3 = (bf16[256,2048]{1,0:T(8,128)(2,1)S(1)}, bf16[256,2048]{1,0:T(8,128)(2,1)}, u32[]{:S(2)}) copy-start(bf16[256,2048]{1,0:T(8,128)(2,1)} %param.25) | copy-start | bytes 3145732
  245.4 5.2 %copy-start.49 = (f32[256]{0:T(256)S(1)}, f32[256]{0:T(256)}, u32[]{:S(2)}) copy-start(f32[256]{0:T(256)} %copy-done.47) | copy-start | bytes 3076
  245.4 5.2 %copy-start.53 = (f32[2048]{0:T(1024)S(1)}, f32[2048]{0:T(1024)}, u32[]{:S(2)}) copy-start(f32[2048]{0:T(1024)} %param.26) | copy-start | bytes 24580
  252.5 5.8 %copy-start.50 = (f32[128]{0:T(128)S(1)}, f32[128]{0:T(128)}, u32[]{:S(2)}) copy-start(f32[128]{0:T(128)} %param.34) | copy-start | bytes 1540
  254.6 4.7 %collective-permute-start = (bf16[15,256]{0,1:T(8,128)(2,1)S(1)}, bf16[15,256]{0,1:T(8,128)(2,1)S(1)}, u32[]{:S(2)}, u32[]{:S(2)}) collective-permute-start(bf16[15,256]{0,1:T(8,128)(2,1)S(1)} %get-tuple-element.639), channel_id=1, source_target_pairs={{0,4},{4,8},{8,12},{1,5},{5,9},{9,13},{2,6},{6,10},{10,14},{3,7},{... | collective-permute-start | bytes 23048 | tf_op jit(solution)/shard_map/ppermute | solution.py:44
  257.1 6.2 %collective-permute-start.1 = (bf16[15,256]{0,1:T(8,128)(2,1)S(1)}, bf16[15,256]{0,1:T(8,128)(2,1)S(1)}, u32[]{:S(2)}, u32[]{:S(2)}) collective-permute-start(bf16[15,256]{0,1:T(8,128)(2,1)S(1)} %get-tuple-element.640), channel_id=1, source_target_pairs={{4,0},{8,4},{12,8},{5,1},{9,5},{13,9},{6,2},{10,6},{14,10},{7,3},{... | collective-permute-start | bytes 23048 | tf_op jit(solution)/shard_map/ppermute | solution.py:47
  258.5 4.9 %copy-start.13 = (f32[1,256]{1,0:T(1,128)S(1)}, f32[1,256]{1,0:T(1,128)}, u32[]{:S(2)}) copy-start(f32[1,256]{1,0:T(1,128)} %get-tuple-element.641) | copy-start | bytes 3076
  258.5 4.9 %copy-start.14 = (f32[1,256]{1,0:T(1,128)S(1)}, f32[1,256]{1,0:T(1,128)}, u32[]{:S(2)}) copy-start(f32[1,256]{1,0:T(1,128)} %get-tuple-element.642) | copy-start | bytes 3076
  258.5 4.9 %copy-start.15 = (f32[1,256]{1,0:T(1,128)S(1)}, f32[1,256]{1,0:T(1,128)}, u32[]{:S(2)}) copy-start(f32[1,256]{1,0:T(1,128)} %get-tuple-element.643) | copy-start | bytes 3076
  258.5 4.9 %copy-start.16 = (f32[1,256]{1,0:T(1,128)S(1)}, f32[1,256]{1,0:T(1,128)}, u32[]{:S(2)}) copy-start(f32[1,256]{1,0:T(1,128)} %get-tuple-element.644) | copy-start | bytes 3076
  258.5 4.9 %copy-start.17 = (f32[1,256]{1,0:T(1,128)S(1)}, f32[1,256]{1,0:T(1,128)}, u32[]{:S(2)}) copy-start(f32[1,256]{1,0:T(1,128)} %get-tuple-element.645) | copy-start | bytes 3076
  258.5 4.9 %copy-start.18 = (f32[1,256]{1,0:T(1,128)S(1)}, f32[1,256]{1,0:T(1,128)}, u32[]{:S(2)}) copy-start(f32[1,256]{1,0:T(1,128)} %get-tuple-element.646) | copy-start | bytes 3076
  258.5 4.9 %copy-start.19 = (f32[1,256]{1,0:T(1,128)S(1)}, f32[1,256]{1,0:T(1,128)}, u32[]{:S(2)}) copy-start(f32[1,256]{1,0:T(1,128)} %get-tuple-element.647) | copy-start | bytes 3076
  258.5 4.9 %copy-start.20 = (f32[1,256]{1,0:T(1,128)S(1)}, f32[1,256]{1,0:T(1,128)}, u32[]{:S(2)}) copy-start(f32[1,256]{1,0:T(1,128)} %get-tuple-element.648) | copy-start | bytes 3076
  258.5 4.9 %copy-start.21 = (f32[1,256]{1,0:T(1,128)S(1)}, f32[1,256]{1,0:T(1,128)}, u32[]{:S(2)}) copy-start(f32[1,256]{1,0:T(1,128)} %get-tuple-element.649) | copy-start | bytes 3076
  258.6 4.9 %copy-start.22 = (f32[1,256]{1,0:T(1,128)S(1)}, f32[1,256]{1,0:T(1,128)}, u32[]{:S(2)}) copy-start(f32[1,256]{1,0:T(1,128)} %get-tuple-element.650) | copy-start | bytes 3076
  258.6 4.9 %copy-start.23 = (f32[1,256]{1,0:T(1,128)S(1)}, f32[1,256]{1,0:T(1,128)}, u32[]{:S(2)}) copy-start(f32[1,256]{1,0:T(1,128)} %get-tuple-element.651) | copy-start | bytes 3076
  258.6 4.9 %copy-start.24 = (f32[1,256]{1,0:T(1,128)S(1)}, f32[1,256]{1,0:T(1,128)}, u32[]{:S(2)}) copy-start(f32[1,256]{1,0:T(1,128)} %get-tuple-element.652) | copy-start | bytes 3076
  258.6 4.9 %copy-start.25 = (f32[1,256]{1,0:T(1,128)S(1)}, f32[1,256]{1,0:T(1,128)}, u32[]{:S(2)}) copy-start(f32[1,256]{1,0:T(1,128)} %get-tuple-element.653) | copy-start | bytes 3076
  258.6 4.9 %copy-start.26 = (f32[1,256]{1,0:T(1,128)S(1)}, f32[1,256]{1,0:T(1,128)}, u32[]{:S(2)}) copy-start(f32[1,256]{1,0:T(1,128)} %get-tuple-element.654) | copy-start | bytes 3076
  258.6 4.9 %copy-start.27 = (f32[1,256]{1,0:T(1,128)S(1)}, f32[1,256]{1,0:T(1,128)}, u32[]{:S(2)}) copy-start(f32[1,256]{1,0:T(1,128)} %get-tuple-element.655) | copy-start | bytes 3076
  258.6 4.9 %copy-start.28 = (f32[1,256]{1,0:T(1,128)S(1)}, f32[1,256]{1,0:T(1,128)}, u32[]{:S(2)}) copy-start(f32[1,256]{1,0:T(1,128)} %get-tuple-element.656) | copy-start | bytes 3076
  258.6 4.9 %copy-start.29 = (f32[1,256]{1,0:T(1,128)S(1)}, f32[1,256]{1,0:T(1,128)}, u32[]{:S(2)}) copy-start(f32[1,256]{1,0:T(1,128)} %get-tuple-element.657) | copy-start | bytes 3076
  258.6 4.9 %copy-start.30 = (f32[1,256]{1,0:T(1,128)S(1)}, f32[1,256]{1,0:T(1,128)}, u32[]{:S(2)}) copy-start(f32[1,256]{1,0:T(1,128)} %get-tuple-element.658) | copy-start | bytes 3076
  258.6 4.9 %copy-start.31 = (f32[1,256]{1,0:T(1,128)S(1)}, f32[1,256]{1,0:T(1,128)}, u32[]{:S(2)}) copy-start(f32[1,256]{1,0:T(1,128)} %get-tuple-element.659) | copy-start | bytes 3076
  263.7 9.3 %copy-start.45 = (f32[256]{0:T(256)S(1)}, f32[256]{0:T(256)}, u32[]{:S(2)}) copy-start(f32[256]{0:T(256)} %param.37) | copy-start | bytes 3076
  263.7 9.2 %copy-start.46 = (f32[256]{0:T(256)S(1)}, f32[256]{0:T(256)}, u32[]{:S(2)}) copy-start(f32[256]{0:T(256)} %param.36) | copy-start | bytes 3076
  (14 other events, 66.2 us)
Sparse Core Ops, SparseCore 0:
  8.9 30.8 all-gather.9
  41.4 27.5 all-gather.11
  70.5 27.4 all-gather.13
  99.5 27.1 all-gather.15
  128.1 31.9 all-gather.17
  275.9 24.8 reduce-scatter.1
where the time goes:
time: 309 us; the launch traced here: 308 us
  other arithmetic  85.9 us (28%)
  blocking collectives  80.4 us (26%)
  matrix products  54.7 us (18%)
  waiting for transfers between devices  52.2 us (17%)
  local copies, waits for them, and re-layouts  14.9 us (5%)
  between operations  14.7 us (5%)
  starting transfers between devices  4.01 us (1%)
    another operation x5, other arithmetic, block_terms(): jax.scipy.linalg.solve_triangular(identity + lower_part, jnp.broadcast_to...  78.7 us
    all_gather x4, blocking collectives, entering(): lax.all_gather(part.astype(kind), axis)  59.8 us
    dot_general x82, matrix products, high_dot(): return jnp.matmul(left, right, precision=PRECISE)  39.7 us
    reduce_scatter x1, waiting for transfers between devices, on_device(): lax.psum_scatter(term.astype(jnp.bfloat16), 'tp', scatter_dimension=1, ti...  25.1 us
    all_gather x1, blocking collectives, on_device(): lax.all_gather(w_gates, 'sp', axis=0, tiled=True)  14.9 us
    all_gather x1, waiting for transfers between devices, on_device(): lax.all_gather(w_query, 'sp', axis=0, tiled=True)  10.9 us
    dot_general x6, matrix products, on_device(): jnp.dot(normed, rows_here, preferred_element_type=jnp.float32)  10.5 us
    all_gather x1, waiting for transfers between devices, on_device(): lax.all_gather(w_key, 'sp', axis=0, tiled=True)  9.11 us
  transfers between devices with their start and end apart: 8, of which 4 were waited for; matrix products, arithmetic and copies ran while one was open for 48% of the time, Pallas kernels for 0%

commit v1 on v0

v1 whole, which is shorter than its diff:
```python
import functools

import jax
import jax.numpy as jnp
from jax import lax
from jax.experimental import pallas as pl
from jax.experimental.pallas import tpu as pltpu
from jax.sharding import PartitionSpec as P

EPSILON = 1e-06
BETA_SHIFT = 6.0
HALO = 16
MESH = pl.DeviceIdType.MESH
F32 = jnp.float32
BF16 = jnp.bfloat16
NT = (((1,), (1,)), ((), ()))
TN = (((0,), (0,)), ((), ()))
NN = (((1,), (0,)), ((), ()))
KEY, GATE, VALUE, QUERY, GLU, OPEN = range(6)


def bdot(left, right, dims=NN):
    return lax.dot_general(
        left.astype(BF16), right.astype(BF16), dims, preferred_element_type=F32
    )


def each(count, action):
    if count <= 8:
        for step in range(count):
            action(step)
    else:
        def body(step, carry):
            action(step)
            return carry

        lax.fori_loop(0, count, body, 0)


def kernel(cfg, tok_h, gain, wk_h, wg_h, wv_h, wq_h, wa_h, wb_h, ld, ldt, hgain, ck, ng, ns, od_h, oc_h,
           out,
           tok, normed, wk, wg, wv, wq, wa, wb, od, oc,
           keys, vals, betas, cums, xinv, gaps, rhs, local_out, reads, maps, ends,
           chain_in, chain_out, glu, halo, pad, conv, stat_out, stat_in, conv_acc, part_out, part_in,
           local_sem, z_send, z_recv, y_send, y_recv, chain_send, chain_recv,
           halo_send, halo_recv, stat_send, stat_recv, part_send, part_recv):
    n_grp, n_sp, n_tp, conv_total = cfg
    grp, sp, tp = lax.axis_index("grp"), lax.axis_index("sp"), lax.axis_index("tp")
    length, width = tok.shape
    rows = wk_h.shape[0]
    channels = wa.shape[1]
    head_width = hgain.shape[1]
    heads = wk.shape[1] // head_width
    share = (rows * 3 // 8) // 16 * 16 if n_grp == 2 else 0
    pulled = rows - share

    sources = (wk_h, wg_h, wv_h, wq_h, wa_h, wb_h)
    targets = (wk, wg, wv, wq, wa, wb)

    def block_of(w, index, start, count):
        if w == GATE:
            return targets[w].at[index]
        return targets[w].at[pl.ds(pl.multiple_of(index * rows + start, 16), count)]

    load_tok = pltpu.make_async_copy(tok_h, tok, local_sem.at[0])
    load_tok.start()
    own = [
        pltpu.make_async_copy(sources[w], block_of(w, sp, 0, rows), local_sem.at[1 + w])
        for w in range(6)
    ]
    for copy in own:
        copy.start()
    load_od = pltpu.make_async_copy(od_h, od, local_sem.at[7])
    load_oc = pltpu.make_async_copy(oc_h, oc, local_sem.at[8])

    barrier = pltpu.get_barrier_semaphore()

    def greet(axis, me, count):
        def one(step):
            pl.semaphore_signal(
                barrier, inc=1, device_id={axis: lax.rem(me + step + 1, count)}, device_id_type=MESH
            )

        each(count - 1, one)

    greet("sp", sp, n_sp)
    greet("tp", tp, n_tp)
    greet("grp", grp, n_grp)
    pl.semaphore_wait(barrier, n_sp + n_tp + n_grp - 3)

    def z_copy(w, step):
        dest = lax.rem(sp + step + 1, n_sp)
        if w == GATE:
            source, target = sources[w], block_of(w, sp, 0, 0)
        else:
            start = pl.multiple_of(grp * share, 16) if share else 0
            source = sources[w].at[pl.ds(start, pulled)]
            target = block_of(w, sp, start, pulled)
        return pltpu.make_async_remote_copy(
            src_ref=source, dst_ref=target,
            send_sem=z_send.at[w, step], recv_sem=z_recv.at[w, step],
            device_id={"sp": dest}, device_id_type=MESH,
        )

    def z_arrival(w, step):
        source = lax.rem(sp + n_sp - step - 1, n_sp)
        if w == GATE:
            place = block_of(w, source, 0, 0)
        else:
            place = block_of(w, source, pl.multiple_of(grp * share, 16) if share else 0, pulled)
        return pltpu.make_async_remote_copy(
            src_ref=place, dst_ref=place,
            send_sem=z_send.at[w, step], recv_sem=z_recv.at[w, step],
            device_id={"sp": source}, device_id_type=MESH,
        )

    def y_copy(w, step):
        source = lax.rem(sp + n_sp - step - 1, n_sp)
        place = block_of(w, source, pl.multiple_of(grp * pulled, 16), share)
        return pltpu.make_async_remote_copy(
            src_ref=place, dst_ref=place,
            send_sem=y_send.at[w, step], recv_sem=y_recv.at[w, step],
            device_id={"grp": 1 - grp}, device_id_type=MESH,
        )

    def y_arrival(w, step):
        source = lax.rem(sp + n_sp - step - 1, n_sp)
        place = block_of(w, source, pl.multiple_of((1 - grp) * pulled, 16), share)
        return pltpu.make_async_remote_copy(
            src_ref=place, dst_ref=place,
            send_sem=y_send.at[w, step], recv_sem=y_recv.at[w, step],
            device_id={"grp": 1 - grp}, device_id_type=MESH,
        )

    for w in range(6):
        each(n_sp - 1, lambda step, w=w: z_copy(w, step).start())

    load_od.start()
    load_oc.start()

    def relay(w):
        def one(step):
            z_arrival(w, step).wait_recv()
            if share and w != GATE:
                y_copy(w, step).start()

        each(n_sp - 1, one)

    def complete(w):
        own[w].wait()
        if share and w != GATE:
            each(n_sp - 1, lambda step: y_arrival(w, step).wait_recv())

    load_tok.wait()
    chunk = 64
    for at in range(0, length, chunk):
        here = tok[at:at + chunk, :].astype(F32)
        scale = lax.rsqrt(jnp.mean(here * here, axis=-1, keepdims=True) + EPSILON)
        normed[at:at + chunk, :] = (here * scale * gain[...]).astype(BF16)

    def project(w):
        return jnp.dot(normed[...], targets[w][...], preferred_element_type=F32)

    def unit_rows(tensor):
        return tensor * lax.rsqrt(jnp.sum(tensor * tensor, axis=-1, keepdims=True) + EPSILON)

    def silu(tensor):
        return tensor * jax.nn.sigmoid(tensor)

    relay(KEY)
    relay(GATE)
    complete(GATE)
    gate_cols = jnp.zeros((length, 4 * heads), F32)
    gate_rows = jnp.zeros((4 * heads, length), F32)
    for index in range(n_sp):
        normed_part = normed[:, index * rows:(index + 1) * rows]
        gate_cols = gate_cols + lax.dot_general(normed_part, wg[index], NT, preferred_element_type=F32)
        gate_rows = gate_rows + lax.dot_general(wg[index], normed_part, NT, preferred_element_type=F32)

    row_at = lax.broadcasted_iota(jnp.int32, (length, length), 0)
    col_at = lax.broadcasted_iota(jnp.int32, (length, length), 1)

    complete(KEY)
    key_proj = silu(project(KEY))
    pairs = [(h, r) for h in range(heads) for r in range(2)]
    for h in range(heads):
        keys[h] = unit_rows(key_proj[:, h * head_width:(h + 1) * head_width])
    lowers = [None] * len(pairs)
    for h in range(heads):
        grams = bdot(keys[h], keys[h], NT)
        for r in range(2):
            p = 2 * h + r
            decay_col = ld[:, p:p + 1] * (0.5 + jax.nn.sigmoid(gate_cols[:, 2 * p:2 * p + 1]))
            decay_row = ldt[p:p + 1, :] * (0.5 + jax.nn.sigmoid(gate_rows[2 * p:2 * p + 1, :]))
            beta = jax.nn.sigmoid(gate_cols[:, 2 * p + 1:2 * p + 2] - BETA_SHIFT)
            if r == 0:
                seen_down, seen_across = row_at <= col_at, col_at <= row_at
            else:
                seen_down, seen_across = row_at >= col_at, col_at >= row_at
            cum_row = jnp.sum(jnp.where(seen_down, decay_col, 0.0), axis=0, keepdims=True)
            cum_col = jnp.sum(jnp.where(seen_across, decay_row, 0.0), axis=1, keepdims=True)
            weighting = jnp.where(
                seen_across, jnp.exp(jnp.where(seen_across, cum_col - cum_row, 0.0)), 0.0
            )
            gaps[p] = weighting
            betas[p] = jnp.broadcast_to(beta, (length, head_width))
            cums[p] = jnp.broadcast_to(cum_col, (length, head_width))
            lower = jnp.where(row_at != col_at, grams * weighting * beta, 0.0)
            rhs[p] = lower
            near = (row_at // 2 == col_at // 2)
            xinv[p] = jnp.where(row_at == col_at, 1.0, jnp.where(near, -lower, 0.0))

    size = 2
    while size < length:
        inside = (row_at // (2 * size) == col_at // (2 * size)) & (row_at // size != col_at // size)
        for p in range(len(pairs)):
            across = jnp.where(inside, rhs[p], 0.0)
            inverse = xinv[p]
            xinv[p] = inverse - bdot(inverse, bdot(across, inverse))
        if size == 8:
            relay(VALUE)
        size *= 2

    complete(VALUE)
    value_proj = silu(project(VALUE))
    eye = (
        lax.broadcasted_iota(jnp.int32, (head_width, head_width), 0)
        == lax.broadcasted_iota(jnp.int32, (head_width, head_width), 1)
    )
    for h, r in pairs:
        p = 2 * h + r
        beta, cum, key = betas[p], cums[p], keys[h]
        value = value_proj[:, h * head_width:(h + 1) * head_width]
        total = cum[length - 1:length, :] if r == 0 else cum[0:1, :]
        right = jnp.concatenate([beta * value, beta * key * jnp.exp(cum)], axis=1)
        solved = bdot(xinv[p], right)
        vals[p] = solved.astype(BF16)
        passed = bdot(key * jnp.exp(total - cum), solved, TN)
        ends[p] = passed[:, :head_width]
        maps[p] = (jnp.where(eye, jnp.exp(total), 0.0) - passed[:, head_width:]).astype(BF16)

    def place_of(r):
        return sp if r == 0 else n_sp - 1 - sp

    def chain_copy(r):
        dest = lax.rem(sp + 1, n_sp) if r == 0 else lax.rem(sp + n_sp - 1, n_sp)
        return pltpu.make_async_remote_copy(
            src_ref=chain_out.at[r], dst_ref=chain_in.at[r],
            send_sem=chain_send.at[r], recv_sem=chain_recv.at[r],
            device_id={"sp": dest}, device_id_type=MESH,
        )

    def chain_point(low, high):
        for r in range(2):
            at = place_of(r)

            @pl.when((at >= low) & (at <= high))
            def _(r=r, at=at):
                if low == 0:
                    for h in range(heads):
                        chain_in[r, h] = jnp.zeros((head_width, head_width), BF16)
                        chain_out[r, h] = ends[2 * h + r].astype(BF16)
                else:
                    chain_copy(r).wait_recv()
                    for h in range(heads):
                        p = 2 * h + r
                        chain_out[r, h] = (bdot(maps[p], chain_in[r, h]) + ends[p]).astype(BF16)

                @pl.when(at < n_sp - 1)
                def _():
                    chain_copy(r).start()

    chain_point(0, 0)
    relay(QUERY)
    complete(QUERY)
    query_proj = silu(project(QUERY))
    for h in range(heads):
        query = unit_rows(query_proj[:, h * head_width:(h + 1) * head_width]) * head_width ** -0.5
        scores = bdot(query, keys[h], NT)
        for r in range(2):
            p = 2 * h + r
            both = jnp.dot((scores * gaps[p]).astype(BF16), vals[p], preferred_element_type=F32)
            reads[p] = (query * jnp.exp(cums[p]) - both[:, head_width:]).astype(BF16)
            if r == 0:
                local_out[h] = both[:, :head_width]
            else:
                local_out[h] = local_out[h] + both[:, :head_width]
    chain_point(1, 1)
    relay(GLU)
    chain_point(2, 2)
    relay(OPEN)
    complete(GLU)
    glu_proj = project(GLU)
    chain_point(3, n_sp - 1)
    complete(OPEN)
    gated = (glu_proj * jax.nn.sigmoid(project(OPEN))).astype(BF16)
    glu[...] = gated
    pad[HALO:HALO + length, :] = gated.astype(F32)

    def halo_copy(r):
        start = length - HALO if r == 0 else 0
        dest = lax.rem(sp + 1, n_sp) if r == 0 else lax.rem(sp + n_sp - 1, n_sp)
        return pltpu.make_async_remote_copy(
            src_ref=glu.at[pl.ds(start, HALO)], dst_ref=halo.at[r],
            send_sem=halo_send.at[r], recv_sem=halo_recv.at[r],
            device_id={"sp": dest}, device_id_type=MESH,
        )

    for r in range(2):
        @pl.when(place_of(r) < n_sp - 1)
        def _(r=r):
            halo_copy(r).start()
    for r in range(2):
        start = 0 if r == 0 else HALO + length

        @pl.when(place_of(r) > 0)
        def _(r=r, start=start):
            halo_copy(r).wait_recv()
            pad[start:start + HALO, :] = halo[r].astype(F32)

        @pl.when(place_of(r) == 0)
        def _(start=start):
            pad[start:start + HALO, :] = jnp.zeros((HALO, channels), F32)

    taps = ck.shape[0]
    for at in range(0, length, chunk):
        first = at + HALO - taps // 2
        total = pad[first:first + chunk, :] * ck[0:1, :]
        for j in range(1, taps):
            total = total + pad[first + j:first + j + chunk, :] * ck[j:j + 1, :]
        conv[at:at + chunk, :] = total
    filtered = conv[...]
    sum_col = jnp.sum(filtered, axis=-1, keepdims=True)
    square_col = jnp.sum(filtered * filtered, axis=-1, keepdims=True)
    same = row_at == col_at
    stat_out[...] = jnp.zeros(stat_out.shape, F32)
    stat_out[0:1, :] = jnp.sum(jnp.where(same, sum_col, 0.0), axis=0, keepdims=True)
    stat_out[1:2, :] = jnp.sum(jnp.where(same, square_col, 0.0), axis=0, keepdims=True)

    def stat_copy(step):
        return pltpu.make_async_remote_copy(
            src_ref=stat_out, dst_ref=stat_in.at[step],
            send_sem=stat_send.at[step], recv_sem=stat_recv.at[step],
            device_id={"tp": lax.rem(tp + step + 1, n_tp)}, device_id_type=MESH,
        )

    for step in range(n_tp - 1):
        stat_copy(step).start()

    joined_heads = []
    for h in range(heads):
        joined = local_out[h] + jnp.dot(reads[2 * h], chain_in[0, h], preferred_element_type=F32)
        joined = joined + jnp.dot(reads[2 * h + 1], chain_in[1, h], preferred_element_type=F32)
        scale = lax.rsqrt(jnp.mean(joined * joined, axis=-1, keepdims=True) + EPSILON)
        joined_heads.append((joined * scale * hgain[...]).astype(BF16))
    delta_mix = jnp.concatenate(joined_heads, axis=1) if heads > 1 else joined_heads[0]
    load_od.wait()
    load_oc.wait()
    columns = width // n_tp
    order = [(step + n_tp // 2) % n_tp for step in range(n_tp)]
    order = [o for o in order if o] + [0]

    def rows_of(matrix, o):
        dest = lax.rem(tp + o, n_tp)
        return matrix[pl.ds(pl.multiple_of(dest * columns, 16), columns), :]

    for o in order:
        conv_acc[o] = lax.dot_general(delta_mix, rows_of(od, o), NT, preferred_element_type=F32)

    stats = stat_out[0:2, :]
    for step in range(n_tp - 1):
        stat_copy(step).wait_recv()
        stats = stats + stat_in[step, 0:2, :]
    center = jnp.sum(jnp.where(same, stats[0:1, :], 0.0), axis=1, keepdims=True) / conv_total
    squares = jnp.sum(jnp.where(same, stats[1:2, :], 0.0), axis=1, keepdims=True) / conv_total
    spread = squares - center * center
    normal = (filtered - center) * lax.rsqrt(spread + EPSILON)
    conv_mix = silu(normal * ng[...] + ns[...]).astype(BF16)

    def part_copy(o):
        return pltpu.make_async_remote_copy(
            src_ref=part_out.at[o - 1], dst_ref=part_in.at[o - 1],
            send_sem=part_send.at[o - 1], recv_sem=part_recv.at[o - 1],
            device_id={"tp": lax.rem(tp + o, n_tp)}, device_id_type=MESH,
        )

    for o in order:
        term = conv_acc[o] + lax.dot_general(conv_mix, rows_of(oc, o), NT, preferred_element_type=F32)
        if o:
            part_out[o - 1] = term.astype(BF16)
            part_copy(o).start()
        else:
            result = term.astype(BF16).astype(F32)
    for o in range(1, n_tp):
        part_copy(o).wait_recv()
        result = result + part_in[o - 1].astype(F32)
    out[...] = result.astype(BF16)

    for w in range(6):
        each(n_sp - 1, lambda step, w=w: z_copy(w, step).wait_send())
        if share and w != GATE:
            each(n_sp - 1, lambda step, w=w: y_copy(w, step).wait_send())
    for r in range(2):
        @pl.when(place_of(r) < n_sp - 1)
        def _(r=r):
            chain_copy(r).wait_send()
            halo_copy(r).wait_send()
    for step in range(n_tp - 1):
        stat_copy(step).wait_send()
        part_copy(step + 1).wait_send()


def solution(mesh):
    n_grp, n_sp, n_tp = mesh.shape["grp"], mesh.shape["sp"], mesh.shape["tp"]

    def on_device(tokens_in, input_gain, w_query, w_key, w_value, w_gates, w_glu_value,
                  sigmoid_opener_matrix, log_decay, head_gain, conv_kernel, norm_gain, norm_shift,
                  out_delta, out_conv):
        length, width = tokens_in.shape
        head_width = head_gain.shape[0]
        head_cols = w_query.shape[1]
        heads = head_cols // head_width
        channels = w_glu_value.shape[1]
        rows = w_query.shape[0]
        pairs = 2 * heads
        columns = width // n_tp
        dma, vmem = pltpu.SemaphoreType.DMA, pltpu.VMEM
        anywhere = pl.BlockSpec(memory_space=pltpu.HBM)
        inside = pl.BlockSpec(memory_space=pltpu.VMEM)
        scratch = [
            vmem((length, width), BF16), vmem((length, width), BF16),
            vmem((width, head_cols), BF16), vmem((n_sp, 4 * heads, rows), BF16),
            vmem((width, head_cols), BF16), vmem((width, head_cols), BF16),
            vmem((width, channels), BF16), vmem((width, channels), BF16),
            vmem((width, head_cols), BF16), vmem((width, channels), BF16),
            vmem((heads, length, head_width), F32), vmem((pairs, length, 2 * head_width), BF16),
            vmem((pairs, length, head_width), F32), vmem((pairs, length, head_width), F32),
            vmem((pairs, length, length), F32), vmem((pairs, length, length), F32),
            vmem((pairs, length, length), F32),
            vmem((heads, length, head_width), F32), vmem((pairs, length, head_width), BF16),
            vmem((pairs, head_width, head_width), BF16), vmem((pairs, head_width, head_width), F32),
            vmem((2, heads, head_width, head_width), BF16), vmem((2, heads, head_width, head_width), BF16),
            vmem((length, channels), BF16), vmem((2, HALO, channels), BF16),
            vmem((length + 2 * HALO, channels), F32), vmem((length, channels), F32),
            vmem((8, length), F32), vmem((n_tp - 1, 8, length), F32),
            vmem((n_tp, length, columns), F32),
            vmem((n_tp - 1, length, columns), BF16), vmem((n_tp - 1, length, columns), BF16),
            dma((9,)),
            dma((6, n_sp - 1)), dma((6, n_sp - 1)), dma((6, n_sp - 1)), dma((6, n_sp - 1)),
            dma((2,)), dma((2,)), dma((2,)), dma((2,)),
            dma((n_tp - 1,)), dma((n_tp - 1,)), dma((n_tp - 1,)), dma((n_tp - 1,)),
        ]
        return pl.pallas_call(
            functools.partial(kernel, (n_grp, n_sp, n_tp, float(channels * n_tp))),
            out_shape=jax.ShapeDtypeStruct((length, columns), BF16),
            in_specs=[anywhere, inside] + [anywhere] * 6 + [inside] * 6 + [anywhere] * 2,
            out_specs=inside,
            scratch_shapes=scratch,
            compiler_params=pltpu.CompilerParams(
                collective_id=0, has_side_effects=True, vmem_limit_bytes=60 * 1024 * 1024
            ),
        )(
            tokens_in, input_gain.reshape(1, width), w_key, w_gates.T, w_value, w_query,
            w_glu_value, sigmoid_opener_matrix, log_decay, log_decay.T,
            head_gain.reshape(1, head_width), conv_kernel, norm_gain.reshape(1, channels),
            norm_shift.reshape(1, channels), out_delta, out_conv,
        )

    placed = (
        P(("grp", "sp"), None), P(), P("sp", "tp"), P("sp", "tp"), P("sp", "tp"), P("sp", "tp"),
        P("sp", "tp"), P("sp", "tp"), P(("grp", "sp"), "tp"), P(), P(None, "tp"), P("tp"), P("tp"),
        P(None, "tp"), P(None, "tp"),
    )
    return jax.shard_map(
        on_device, mesh=mesh, in_specs=placed, out_specs=P(("grp", "sp"), "tp"), check_vma=False
    )
```

time: 309 us -> 114 us (0.37)
  Pallas kernels: 0 us -> 110 us
  other arithmetic: 85.9 us -> 0 us
  blocking collectives: 80.4 us -> 0 us
  matrix products: 54.7 us -> 0 us
  waiting for transfers between devices: 52.2 us -> 0 us
  between operations: 14.7 us -> 0.01 us
  local copies, waits for them, and re-layouts: 14.9 us -> 3.16 us
  starting transfers between devices: 4.01 us -> 0 us
    pallas_call x0 -> x1, Pallas kernels: none -> 110 us  [on_device(): pl.pallas_call(functools.partial(kernel, (n_grp, n_sp, n_tp, float(channe...]
    another operation x7 -> x0, other arithmetic: 79.7 us -> none  [the longest x5 78.7 us: block_terms(): jax.scipy.linalg.solve_triangular(identity + lower_part, jnp.broadcast_to...]
    all_gather x5 -> x0, blocking collectives: 74.7 us -> none  [the longest x4 59.8 us: entering(): lax.all_gather(part.astype(kind), axis)]
    dot_general x90 -> x0, matrix products: 53.5 us -> none  [the longest x82 39.7 us: high_dot(): return jnp.matmul(left, right, precision=PRECISE)]
    reduce_scatter x1 -> x0, waiting for transfers between devices: 25.1 us -> none  [on_device(): lax.psum_scatter(term.astype(jnp.bfloat16), 'tp', scatter_dimension=1, ti...]
    all_gather x5 -> x0, waiting for transfers between devices: 20.1 us -> none  [the longest x1 10.9 us: on_device(): lax.all_gather(w_query, 'sp', axis=0, tiled=True)]
    psum x1 -> x0, blocking collectives: 5.67 us -> none  [conv_branch(): lax.psum((jnp.sum(conv_rows, axis=-1), jnp.sum(conv_rows * conv_rows, axi...]
    mul x10 -> x0, local copies, waits for them, and re-layouts: 5.61 us -> none  [the longest x8 5.44 us: advance(): state_now * end_decay[:, None, None]]
  transfers between devices with their start and end apart: 8 -> 0, of which waited for: 4 -> 0; matrix products, arithmetic and copies ran while one was open for 48% -> 0% of each run, Pallas kernels for 0% -> 0%
where the time goes in v1:
time: 114 us; the launch traced here: 113 us
  Pallas kernels  110 us (96%)
  local copies, waits for them, and re-layouts  3.16 us (3%)
    pallas_call x1, Pallas kernels, on_device(): pl.pallas_call(functools.partial(kernel, (n_grp, n_sp, n_tp, float(channe...  110 us
    unnamed x4, local copies, waits for them, and re-layouts  3.16 us

profile of v1, /device:TPU:0, one launch (start us, length us, event | category | flops | bytes accessed | tf_op | source)
XLA Modules:
  0.0 113.5 jit_solution(624218565470644615)
XLA Ops:
  0.0 0.0 copy-start
  0.0 0.7 copy-done
  0.7 0.8 copy.16.ld
  1.5 110.3 %shard_map.145 = bf16[256,512]{1,0:T(8,128)(2,1)} custom-call(bf16[256,2048]{1,0:T(8,128)(2,1)} %tok_h.1, f32[1,2048]{1,0:T(1,128)} %bitcast.7, bf16[512,256]{1,0:T(8,128)(2,1)} %wk_h.1, bf16[8,512]{1,0:T(8,128)(2,1)} %bitcast.8, bf16[512,256]{1,0:T(8,128)(2,1)} %wv_h.1, bf16[512,256]{1,0:T(8,128)(2,1)} %wq_h.1, bf16[512,256]{1,0:T(8,128)(2,1)} %wa_h.1, ...), custom_call_target="tpu_custom_call" | custom-call | tf_op jit(solution)/shard_map/pallas_call | solution.py:453
  111.8 1.7 %copy.18 = bf16[256,512]{1,0:T(8,128)(2,1)} copy(bf16[256,512]{1,0:T(8,128)(2,1)} %shard_map.145) | data formatting | bytes 524288
Async XLA Ops:
  0.0 0.7 copy-start

commit v2 on v1

--- a/solution.py
+++ b/solution.py
@@ -51,7 +51,7 @@
     channels = wa.shape[1]
     head_width = hgain.shape[1]
     heads = wk.shape[1] // head_width
-    share = (rows * 3 // 8) // 16 * 16 if n_grp == 2 else 0
+    share = (rows // 2) // 16 * 16 if n_grp == 2 else 0
     pulled = rows - share
 
     sources = (wk_h, wg_h, wv_h, wq_h, wa_h, wb_h)
@@ -88,68 +88,97 @@
     greet("grp", grp, n_grp)
     pl.semaphore_wait(barrier, n_sp + n_tp + n_grp - 3)
 
-    def z_copy(w, step):
-        dest = lax.rem(sp + step + 1, n_sp)
+    def origin(side, d):
+        return sp - d if side == 0 else sp + d
+
+    def arrives(side, d):
+        return sp - d >= 0 if side == 0 else sp + d < n_sp
+
+    def leaves(side, d):
+        if side == 0:
+            return (sp - (d - 1) >= 0) & (sp < n_sp - 1)
+        return (sp + (d - 1) < n_sp) & (sp > 0)
+
+    def part_of(w, index, side_of):
         if w == GATE:
-            source, target = sources[w], block_of(w, sp, 0, 0)
+            return block_of(w, index, 0, 0)
+        if not share:
+            return block_of(w, index, 0, rows)
+        if side_of is None:
+            return block_of(w, index, pl.multiple_of(grp * share, 16), pulled)
+        return block_of(w, index, pl.multiple_of(side_of * pulled, 16), share)
+
+    def z_copy(w, side, d, first=False):
+        target = part_of(w, origin(side, d - 1), None)
+        source = target
+        if first:
+            source = sources[w]
+            if w != GATE and share:
+                source = source.at[pl.ds(pl.multiple_of(grp * share, 16), pulled)]
+        return pltpu.make_async_remote_copy(
+            src_ref=source, dst_ref=target,
+            send_sem=z_send.at[w, side, d - 1], recv_sem=z_recv.at[w, side, d - 1],
+            device_id={"sp": sp + 1 if side == 0 else sp - 1}, device_id_type=MESH,
+        )
+
+    def z_arrival(w, side, d):
+        place = part_of(w, origin(side, d), None)
+        return pltpu.make_async_remote_copy(
+            src_ref=place, dst_ref=place,
+            send_sem=z_send.at[w, side, d - 1], recv_sem=z_recv.at[w, side, d - 1],
+            device_id={"sp": sp + 1 if side == 0 else sp - 1}, device_id_type=MESH,
+        )
+
+    def y_copy(w, side, d, arriving=False):
+        place = part_of(w, origin(side, d), 1 - grp if arriving else grp)
+        return pltpu.make_async_remote_copy(
+            src_ref=place, dst_ref=place,
+            send_sem=y_send.at[w, side, d - 1], recv_sem=y_recv.at[w, side, d - 1],
+            device_id={"grp": 1 - grp}, device_id_type=MESH,
+        )
+
+    def offer(w):
+        for side in range(2):
+            @pl.when(leaves(side, 1))
+            def _(side=side):
+                z_copy(w, side, 1, True).start()
+
+    def relay_hop(w, d):
+        for side in range(2):
+            @pl.when(arrives(side, d))
+            def _(side=side):
+                z_arrival(w, side, d).wait_recv()
+
+                @pl.when(leaves(side, d + 1))
+                def _():
+                    z_copy(w, side, d + 1).start()
+
+                if share and w != GATE:
+                    y_copy(w, side, d).start()
+
+    def relay(w, low=1, high=None):
+        if high is None:
+            each(n_sp - low, lambda step: relay_hop(w, step + low))
         else:
-            start = pl.multiple_of(grp * share, 16) if share else 0
-            source = sources[w].at[pl.ds(start, pulled)]
-            target = block_of(w, sp, start, pulled)
-        return pltpu.make_async_remote_copy(
-            src_ref=source, dst_ref=target,
-            send_sem=z_send.at[w, step], recv_sem=z_recv.at[w, step],
-            device_id={"sp": dest}, device_id_type=MESH,
-        )
-
-    def z_arrival(w, step):
-        source = lax.rem(sp + n_sp - step - 1, n_sp)
-        if w == GATE:
-            place = block_of(w, source, 0, 0)
-        else:
-            place = block_of(w, source, pl.multiple_of(grp * share, 16) if share else 0, pulled)
-        return pltpu.make_async_remote_copy(
-            src_ref=place, dst_ref=place,
-            send_sem=z_send.at[w, step], recv_sem=z_recv.at[w, step],
-            device_id={"sp": source}, device_id_type=MESH,
-        )
-
-    def y_copy(w, step):
-        source = lax.rem(sp + n_sp - step - 1, n_sp)
-        place = block_of(w, source, pl.multiple_of(grp * pulled, 16), share)
-        return pltpu.make_async_remote_copy(
-            src_ref=place, dst_ref=place,
-            send_sem=y_send.at[w, step], recv_sem=y_recv.at[w, step],
-            device_id={"grp": 1 - grp}, device_id_type=MESH,
-        )
-
-    def y_arrival(w, step):
-        source = lax.rem(sp + n_sp - step - 1, n_sp)
-        place = block_of(w, source, pl.multiple_of((1 - grp) * pulled, 16), share)
-        return pltpu.make_async_remote_copy(
-            src_ref=place, dst_ref=place,
-            send_sem=y_send.at[w, step], recv_sem=y_recv.at[w, step],
-            device_id={"grp": 1 - grp}, device_id_type=MESH,
-        )
-
-    for w in range(6):
-        each(n_sp - 1, lambda step, w=w: z_copy(w, step).start())
-
-    load_od.start()
-    load_oc.start()
-
-    def relay(w):
-        def one(step):
-            z_arrival(w, step).wait_recv()
-            if share and w != GATE:
-                y_copy(w, step).start()
-
-        each(n_sp - 1, one)
+            for d in range(low, min(high, n_sp - 1) + 1):
+                relay_hop(w, d)
 
     def complete(w):
         own[w].wait()
         if share and w != GATE:
-            each(n_sp - 1, lambda step: y_arrival(w, step).wait_recv())
+            def one(step):
+                for side in range(2):
+                    @pl.when(arrives(side, step + 1))
+                    def _(side=side):
+                        y_copy(w, side, step + 1, True).wait_recv()
+
+            each(n_sp - 1, one)
+
+    offer(KEY)
+    offer(GATE)
+    offer(VALUE)
+    load_od.start()
+    load_oc.start()
 
     load_tok.wait()
     chunk = 64
@@ -167,8 +196,9 @@
     def silu(tensor):
         return tensor * jax.nn.sigmoid(tensor)
 
+    relay(GATE)
     relay(KEY)
-    relay(GATE)
+    offer(QUERY)
     complete(GATE)
     gate_cols = jnp.zeros((length, 4 * heads), F32)
     gate_rows = jnp.zeros((4 * heads, length), F32)
@@ -185,7 +215,7 @@
     pairs = [(h, r) for h in range(heads) for r in range(2)]
     for h in range(heads):
         keys[h] = unit_rows(key_proj[:, h * head_width:(h + 1) * head_width])
-    lowers = [None] * len(pairs)
+    relay(VALUE, 1, 1)
     for h in range(heads):
         grams = bdot(keys[h], keys[h], NT)
         for r in range(2):
@@ -217,8 +247,13 @@
             across = jnp.where(inside, rhs[p], 0.0)
             inverse = xinv[p]
             xinv[p] = inverse - bdot(inverse, bdot(across, inverse))
-        if size == 8:
-            relay(VALUE)
+        if size == 2:
+            relay(VALUE, 2)
+            offer(GLU)
+        if size == 32:
+            relay(QUERY, 1, 1)
+        if size == 128:
+            relay(QUERY, 2, 2)
         size *= 2
 
     complete(VALUE)
@@ -271,7 +306,9 @@
                     chain_copy(r).start()
 
     chain_point(0, 0)
-    relay(QUERY)
+    relay(QUERY, 3)
+    offer(OPEN)
+    relay(GLU, 1, 1)
     complete(QUERY)
     query_proj = silu(project(QUERY))
     for h in range(heads):
@@ -286,12 +323,14 @@
             else:
                 local_out[h] = local_out[h] + both[:, :head_width]
     chain_point(1, 1)
-    relay(GLU)
+    relay(GLU, 2, 2)
     chain_point(2, 2)
-    relay(OPEN)
+    relay(GLU, 3)
+    relay(OPEN, 1, 1)
+    chain_point(3, n_sp - 1)
     complete(GLU)
     glu_proj = project(GLU)
-    chain_point(3, n_sp - 1)
+    relay(OPEN, 2)
     complete(OPEN)
     gated = (glu_proj * jax.nn.sigmoid(project(OPEN))).astype(BF16)
     glu[...] = gated
@@ -397,9 +436,18 @@
     out[...] = result.astype(BF16)
 
     for w in range(6):
-        each(n_sp - 1, lambda step, w=w: z_copy(w, step).wait_send())
-        if share and w != GATE:
-            each(n_sp - 1, lambda step, w=w: y_copy(w, step).wait_send())
+        def one(step, w=w):
+            for side in range(2):
+                @pl.when(leaves(side, step + 1))
+                def _(side=side):
+                    z_copy(w, side, step + 1).wait_send()
+
+                if share and w != GATE:
+                    @pl.when(arrives(side, step + 1))
+                    def _(side=side):
+                        y_copy(w, side, step + 1).wait_send()
+
+        each(n_sp - 1, one)
     for r in range(2):
         @pl.when(place_of(r) < n_sp - 1)
         def _(r=r):
@@ -446,7 +494,8 @@
             vmem((n_tp, length, columns), F32),
             vmem((n_tp - 1, length, columns), BF16), vmem((n_tp - 1, length, columns), BF16),
             dma((9,)),
-            dma((6, n_sp - 1)), dma((6, n_sp - 1)), dma((6, n_sp - 1)), dma((6, n_sp - 1)),
+            dma((6, 2, n_sp - 1)), dma((6, 2, n_sp - 1)),
+            dma((6, 2, n_sp - 1)), dma((6, 2, n_sp - 1)),
             dma((2,)), dma((2,)), dma((2,)), dma((2,)),
             dma((n_tp - 1,)), dma((n_tp - 1,)), dma((n_tp - 1,)), dma((n_tp - 1,)),
         ]

time: 114 us -> 88.5 us (0.78)
  the two profiles are of different devices: /device:TPU:0 before, /device:TPU:19 now
where the time goes in v2:
time: 88.5 us; the launch traced here: 88.3 us
  Pallas kernels  85.1 us (96%)
  local copies, waits for them, and re-layouts  3.16 us (4%)
    pallas_call x1, Pallas kernels, on_device(): pl.pallas_call(functools.partial(kernel, (n_grp, n_sp, n_tp, float(channe...  85.1 us
    unnamed x4, local copies, waits for them, and re-layouts  3.16 us

profile of v2, /device:TPU:19, one launch (start us, length us, event | category | flops | bytes accessed | tf_op | source)
XLA Modules:
  0.0 88.3 jit_solution(10044765836930228774)
XLA Ops:
  0.0 0.0 copy-start
  0.0 0.7 copy-done
  0.7 0.8 copy.16.ld
  1.5 85.1 %shard_map.145 = bf16[256,512]{1,0:T(8,128)(2,1)} custom-call(bf16[256,2048]{1,0:T(8,128)(2,1)} %tok_h.1, f32[1,2048]{1,0:T(1,128)} %bitcast.7, bf16[512,256]{1,0:T(8,128)(2,1)} %wk_h.1, bf16[8,512]{1,0:T(8,128)(2,1)} %bitcast.8, bf16[512,256]{1,0:T(8,128)(2,1)} %wv_h.1, bf16[512,256]{1,0:T(8,128)(2,1)} %wq_h.1, bf16[512,256]{1,0:T(8,128)(2,1)} %wa_h.1, ...), custom_call_target="tpu_custom_call" | custom-call | tf_op jit(solution)/shard_map/pallas_call | solution.py:502
  86.6 1.7 %copy.18 = bf16[256,512]{1,0:T(8,128)(2,1)} copy(bf16[256,512]{1,0:T(8,128)(2,1)} %shard_map.145) | data formatting | bytes 524288
Async XLA Ops:
  0.0 0.7 copy-start

commit v3 on v2

--- a/solution.py
+++ b/solution.py
@@ -41,9 +41,9 @@
            out,
            tok, normed, wk, wg, wv, wq, wa, wb, od, oc,
            keys, vals, betas, cums, xinv, gaps, rhs, local_out, reads, maps, ends,
-           chain_in, chain_out, glu, halo, pad, conv, stat_out, stat_in, conv_acc, part_out, part_in,
+           chain_in, chain_out, glu, halo, pad, conv, stat_out, stat_in, conv_acc, part_out, part_in, pair_out, pair_in,
            local_sem, z_send, z_recv, y_send, y_recv, chain_send, chain_recv,
-           halo_send, halo_recv, stat_send, stat_recv, part_send, part_recv):
+           halo_send, halo_recv, stat_send, stat_recv, part_send, part_recv, pair_send, pair_recv):
     n_grp, n_sp, n_tp, conv_total = cfg
     grp, sp, tp = lax.axis_index("grp"), lax.axis_index("sp"), lax.axis_index("tp")
     length, width = tok.shape
@@ -396,15 +396,9 @@
     load_od.wait()
     load_oc.wait()
     columns = width // n_tp
-    order = [(step + n_tp // 2) % n_tp for step in range(n_tp)]
-    order = [o for o in order if o] + [0]
-
-    def rows_of(matrix, o):
-        dest = lax.rem(tp + o, n_tp)
-        return matrix[pl.ds(pl.multiple_of(dest * columns, 16), columns), :]
-
-    for o in order:
-        conv_acc[o] = lax.dot_general(delta_mix, rows_of(od, o), NT, preferred_element_type=F32)
+    for dest in range(n_tp):
+        at = slice(dest * columns, (dest + 1) * columns)
+        conv_acc[dest] = lax.dot_general(delta_mix, od[at, :], NT, preferred_element_type=F32)
 
     stats = stat_out[0:2, :]
     for step in range(n_tp - 1):
@@ -416,23 +410,47 @@
     normal = (filtered - center) * lax.rsqrt(spread + EPSILON)
     conv_mix = silu(normal * ng[...] + ns[...]).astype(BF16)
 
-    def part_copy(o):
-        return pltpu.make_async_remote_copy(
-            src_ref=part_out.at[o - 1], dst_ref=part_in.at[o - 1],
-            send_sem=part_send.at[o - 1], recv_sem=part_recv.at[o - 1],
-            device_id={"tp": lax.rem(tp + o, n_tp)}, device_id_type=MESH,
-        )
-
-    for o in order:
-        term = conv_acc[o] + lax.dot_general(conv_mix, rows_of(oc, o), NT, preferred_element_type=F32)
-        if o:
-            part_out[o - 1] = term.astype(BF16)
-            part_copy(o).start()
+    chip, core = tp // 2, lax.rem(tp, 2)
+    chips = n_tp // 2
+    sibling = chip * 2 + 1 - core
+
+    def there(p, place):
+        return lax.rem(chip + p, chips) * 2 + place
+
+    def term_of(dest):
+        at = pl.ds(pl.multiple_of(dest * columns, 16), columns)
+        return conv_acc[dest] + lax.dot_general(conv_mix, oc[at, :], NT, preferred_element_type=F32)
+
+    def pair_copy(p):
+        return pltpu.make_async_remote_copy(
+            src_ref=pair_out.at[p], dst_ref=pair_in.at[p],
+            send_sem=pair_send.at[p], recv_sem=pair_recv.at[p],
+            device_id={"tp": sibling}, device_id_type=MESH,
+        )
+
+    def part_copy(p):
+        return pltpu.make_async_remote_copy(
+            src_ref=part_out.at[p - 1], dst_ref=part_in.at[p - 1],
+            send_sem=part_send.at[p - 1], recv_sem=part_recv.at[p - 1],
+            device_id={"tp": there(p, core)}, device_id_type=MESH,
+        )
+
+    slots = list(range(1, chips)) + [0]
+    for p in slots:
+        pair_out[p] = term_of(there(p, 1 - core)).astype(BF16)
+        pair_copy(p).start()
+    for p in slots:
+        term = term_of(there(p, core))
+        pair_copy(p).wait_recv()
+        term = term + pair_in[p].astype(F32)
+        if p:
+            part_out[p - 1] = term.astype(BF16)
+            part_copy(p).start()
         else:
-            result = term.astype(BF16).astype(F32)
-    for o in range(1, n_tp):
-        part_copy(o).wait_recv()
-        result = result + part_in[o - 1].astype(F32)
+            result = term
+    for p in range(1, chips):
+        part_copy(p).wait_recv()
+        result = result + part_in[p - 1].astype(F32)
     out[...] = result.astype(BF16)
 
     for w in range(6):
@@ -455,7 +473,10 @@
             halo_copy(r).wait_send()
     for step in range(n_tp - 1):
         stat_copy(step).wait_send()
-        part_copy(step + 1).wait_send()
+    for p in range(chips):
+        pair_copy(p).wait_send()
+        if p:
+            part_copy(p).wait_send()
 
 
 def solution(mesh):
@@ -492,12 +513,14 @@
             vmem((length + 2 * HALO, channels), F32), vmem((length, channels), F32),
             vmem((8, length), F32), vmem((n_tp - 1, 8, length), F32),
             vmem((n_tp, length, columns), F32),
-            vmem((n_tp - 1, length, columns), BF16), vmem((n_tp - 1, length, columns), BF16),
+            vmem((n_tp // 2, length, columns), BF16), vmem((n_tp // 2, length, columns), BF16),
+            vmem((n_tp // 2, length, columns), BF16), vmem((n_tp // 2, length, columns), BF16),
             dma((9,)),
             dma((6, 2, n_sp - 1)), dma((6, 2, n_sp - 1)),
             dma((6, 2, n_sp - 1)), dma((6, 2, n_sp - 1)),
             dma((2,)), dma((2,)), dma((2,)), dma((2,)),
-            dma((n_tp - 1,)), dma((n_tp - 1,)), dma((n_tp - 1,)), dma((n_tp - 1,)),
+            dma((n_tp - 1,)), dma((n_tp - 1,)), dma((n_tp // 2,)), dma((n_tp // 2,)),
+            dma((n_tp // 2,)), dma((n_tp // 2,)),
         ]
         return pl.pallas_call(
             functools.partial(kernel, (n_grp, n_sp, n_tp, float(channels * n_tp))),

time: 88.5 us -> 84.4 us (0.954)
  the two profiles are of different devices: /device:TPU:19 before, /device:TPU:0 now
where the time goes in v3:
time: 84.4 us; the launch traced here: 82.9 us
  Pallas kernels  79.7 us (94%)
  local copies, waits for them, and re-layouts  3.16 us (4%)
    pallas_call x1, Pallas kernels, on_device(): pl.pallas_call(functools.partial(kernel, (n_grp, n_sp, n_tp, float(channe...  79.7 us
    unnamed x4, local copies, waits for them, and re-layouts  3.16 us

profile of v3, /device:TPU:0, one launch (start us, length us, event | category | flops | bytes accessed | tf_op | source)
XLA Modules:
  0.0 82.9 jit_solution(13828135732529340831)
XLA Ops:
  0.0 0.0 copy-start
  0.0 0.7 copy-done
  0.7 0.8 copy.16.ld
  1.5 79.7 %shard_map.145 = bf16[256,512]{1,0:T(8,128)(2,1)} custom-call(bf16[256,2048]{1,0:T(8,128)(2,1)} %tok_h.1, f32[1,2048]{1,0:T(1,128)} %bitcast.7, bf16[512,256]{1,0:T(8,128)(2,1)} %wk_h.1, bf16[8,512]{1,0:T(8,128)(2,1)} %bitcast.8, bf16[512,256]{1,0:T(8,128)(2,1)} %wv_h.1, bf16[512,256]{1,0:T(8,128)(2,1)} %wq_h.1, bf16[512,256]{1,0:T(8,128)(2,1)} %wa_h.1, ...), custom_call_target="tpu_custom_call" | custom-call | tf_op jit(solution)/shard_map/pallas_call | solution.py:525
  81.2 1.7 %copy.18 = bf16[256,512]{1,0:T(8,128)(2,1)} copy(bf16[256,512]{1,0:T(8,128)(2,1)} %shard_map.145) | data formatting | bytes 524288
Async XLA Ops:
  0.0 0.7 copy-start
